TPU v7x, 256 devices: a 4x2x16 block of a 4x16x16 slice. The times are simulated.
256 devices in a mesh: grp: 2 (over y), fs: 32 (over z, core), tp: 4 (over x).
Axes of the slice: x: 4, y: 2, z: 16, core: 2. Of those that a mesh axis runs over, the one named last changes fastest.
The devices are a block of a 4x16x16 slice.
Arguments:
- prompt: bfloat16 [24576, 2048], P(('grp', 'fs')), parts along dimension 0, may hold values from -6 to 6
- routes: int32 [24576, 4], P(('grp', 'fs')), parts along dimension 0, may hold values from 0 to 31, all different within a row; in each aligned block of 384 rows (0 to 383, 384 to 767, ...) at most 60 rows name the same one
- route_weight: float32 [24576, 4], P(('grp', 'fs')), parts along dimension 0, may hold values from 0.2 to 1
- norm_gain: float32 [2048], P('fs'), may hold values from 0.1 to 1.9
- gate_train: float32 [32, 2048, 1024], P(None, 'fs', 'tp'), may hold values from -0.4 to 0.4
- up_train: float32 [32, 2048, 1024], P(None, 'fs', 'tp'), may hold values from -0.4 to 0.4
- down_train: float32 [32, 1024, 2048], P(None, 'fs', 'tp'), may hold values from -0.07 to 0.07
Outputs:
- gate_serve: bfloat16 [64, 2048, 1024], P(('grp', 'fs'), None, 'tp'), parts along dimension 0
- up_serve: bfloat16 [64, 2048, 1024], P(('grp', 'fs'), None, 'tp'), parts along dimension 0
- down_serve: bfloat16 [64, 1024, 2048], P(('grp', 'fs'), 'tp'), parts along dimension 0
- mixed: bfloat16 [24576, 2048], P(('grp', 'fs'), 'tp'), parts along dimension 0
There are 2 independent parts, one for each index of `grp`. A program takes and returns all parts, laid end to end along the dimension named above; an argument that names none is the same for every part. Nothing has to cross between parts.
Inputs may be any that keep to these rules, and one draw needn't show every extreme that they name: `routes`: each row names 4 different experts. Among the rows of one index of fs no expert is named more than 60 times, a bound that some block reaches on some index.
All inputs are finite; a program needn't handle non-finite values.
Results may differ from a plain program's by a relative error of at most 0.012.
Values may be sent and summed in bfloat16 or wider, within the bound.
A program may use at most 128 MiB of HBM per device.

v0:
```python
import jax
import jax.numpy as jnp
from jax import lax
from jax.sharding import Mesh
from jax.sharding import PartitionSpec as P

TOP = 4
FS = ("fs_0", "fs_1")
GRP_FS = ("grp", "fs_0", "fs_1")
LIMIT = 7.0
ALPHA = 1.702
EPS = 1e-06


def in_one_piece(arrays, axis, split_dim, concat_dim, along):
    both = jnp.concatenate(arrays, axis=along)
    out, at, outs = (
        lax.all_to_all(both, axis, split_axis=split_dim, concat_axis=concat_dim, tiled=True),
        0,
        [],
    )
    for a in arrays:
        outs.append(lax.slice_in_dim(out, at, at + a.shape[along], axis=along))
        at += a.shape[along]
    return tuple(outs)


def cut_along(value, dim, devices):
    before, after = (value.shape[:dim], value.shape[dim + 1 :])
    return jnp.moveaxis(value.reshape(*before, devices, -1, *after), dim, 0)


def joined_along(pieces, dim):
    pieces = jnp.moveaxis(pieces, 0, dim)
    dims = pieces.shape
    return pieces.reshape(*dims[:dim], dims[dim] * dims[dim + 1], *dims[dim + 2 :])


def moved_by_axis(pieces, axes, turns):
    inside = pieces.shape[1:]
    out = pieces.reshape(*(lax.axis_size(a) for a in axes), *inside)
    for k in turns:
        out = lax.all_to_all(out, axes[k], k, k, tiled=True)
    return out.reshape(-1, *inside)


def exchange_by_chip(value, groups, turns, split_dim, concat_dim):
    devices = lax.axis_size(groups[0]) * lax.axis_size(groups[1])
    pieces = cut_along(value, split_dim, devices)
    return joined_along(moved_by_axis(pieces, groups, turns), concat_dim)


def shards(prompt, routes, route_weight, norm_gain, gate_train, up_train, down_train):
    gate_cast = (norm_gain[None, :, None] * gate_train).astype(jnp.bfloat16)
    up_cast = (norm_gain[None, :, None] * up_train).astype(jnp.bfloat16)
    down_cast = down_train.astype(jnp.bfloat16)
    gate_mine, up_mine, down_rows = (
        *in_one_piece((gate_cast, up_cast), FS, 0, 1, 2),
        lax.all_to_all(down_cast, FS, split_axis=0, concat_axis=1, tiled=True),
    )
    down_mine = lax.all_to_all(down_rows, "tp", split_axis=1, concat_axis=2, tiled=True)
    tok_rows, width = prompt.shape
    experts = gate_train.shape[0]
    quarter = width // lax.axis_size("tp")
    capacity = min(tok_rows, max(2, 5 * tok_rows * TOP // (4 * experts)))
    values = prompt.astype(jnp.float32)
    normed = (values * lax.rsqrt(jnp.mean(values * values, axis=-1, keepdims=True) + EPS)).astype(
        jnp.bfloat16
    )
    flat_expert = routes.reshape(-1)
    onehot = (flat_expert[:, None] == jnp.arange(experts, dtype=jnp.int32)[None, :]).astype(
        jnp.int32
    )
    earlier = jnp.cumsum(onehot, axis=0) - onehot
    slot_pos = jnp.sum(earlier * onehot, axis=1)
    target = flat_expert * capacity + slot_pos
    source_row = jnp.arange(tok_rows * TOP, dtype=jnp.int32) // TOP
    col_start = lax.axis_index("tp") * quarter
    own_cols = lax.dynamic_slice_in_dim(normed, col_start, quarter, 1)
    outbox = (
        jnp.zeros((experts * capacity, quarter), jnp.bfloat16).at[target].set(own_cols[source_row])
    )
    inbox_part = lax.all_to_all(
        outbox.reshape(experts, capacity, quarter), FS, split_axis=0, concat_axis=1, tiled=True
    )
    inbox = lax.all_gather(inbox_part, "tp", axis=2, tiled=True)
    gate_pre = jnp.einsum("erd,edf->erf", inbox, gate_mine, preferred_element_type=jnp.float32)
    up_pre = jnp.einsum("erd,edf->erf", inbox, up_mine, preferred_element_type=jnp.float32)
    gate_pre = jnp.minimum(gate_pre, LIMIT)
    up_pre = jnp.clip(up_pre, -LIMIT, LIMIT)
    hidden = ((up_pre + 1.0) * gate_pre * jax.nn.sigmoid(ALPHA * gate_pre)).astype(jnp.bfloat16)
    own_width = hidden.shape[2]
    empty = jnp.zeros((hidden.shape[0], hidden.shape[1], down_rows.shape[2]), jnp.float32)
    total = empty
    piece = lax.all_gather(hidden, "tp", axis=2, tiled=True)
    for index in range(piece.shape[2] // own_width):
        cols = piece[:, :, index * own_width : (index + 1) * own_width]
        weight_rows = lax.dynamic_slice_in_dim(down_rows, index * own_width, own_width, 1)
        part = jnp.einsum(
            "erf,efd->erd", cols, weight_rows, preferred_element_type=jnp.float32
        ).astype(jnp.bfloat16)
        total = total + part.astype(jnp.float32)
    summed = total.astype(jnp.bfloat16)
    back = exchange_by_chip(summed, ("fs_0", "fs_1"), (1, 0), 1, 0)
    picked = back.reshape(experts * capacity, quarter)[target].astype(jnp.float32)
    weighted = picked.reshape(tok_rows, TOP, quarter) * route_weight[:, :, None]
    mixed = jnp.sum(weighted, axis=1).astype(jnp.bfloat16)
    return (gate_mine, up_mine, down_mine, mixed)


def solution(mesh):
    finer = Mesh(
        mesh.devices.reshape(mesh.shape["grp"], 16, 2, mesh.shape["tp"]),
        ("grp", "fs_0", "fs_1", "tp"),
    )
    placed = (
        P(GRP_FS, None),
        P(GRP_FS, None),
        P(GRP_FS, None),
        P(FS),
        P(None, FS, "tp"),
        P(None, FS, "tp"),
        P(None, FS, "tp"),
    )
    return jax.shard_map(
        shards,
        mesh=finer,
        in_specs=placed,
        out_specs=(
            P(GRP_FS, None, "tp"),
            P(GRP_FS, None, "tp"),
            P(GRP_FS, "tp", None),
            P(GRP_FS, "tp"),
        ),
        check_vma=False,
    )
```

profile of v0, /device:TPU:40, one launch (start us, length us, event | category | flops | bytes accessed | tf_op | source)
XLA Modules:
  0.0 537.3 jit_solution(2255770798606577626)
XLA Ops:
  10.8 15.9 %reduce-window.6 = s32[32,12,128]{2,1,0:T(8,128)S(1)} reduce-window(s32[32,12,128]{2,1,0:T(8,128)} %fusion.28, s32[]{:T(128)} %constant.22.clone.1), window={size=1x1x128 pad=0_0x0_0x127_0}, to_apply=%region_0.0 | reduce-window | flops 6242304 | bytes 393220 | tf_op jit(solution)/shard_map/reduce-window
  31.7 15.8 %scatter_custom_fusion = bf16[1920,512]{1,0:T(8,128)(2,1)} fusion(s32[1536]{0:T(1024)S(1)} %fusion.32, bf16[384,512]{1,0:T(8,128)(2,1)S(1)} %fusion.27, s32[2048]{0:T(1024)} %pad_clamp_fusion.1, bf16[]{:T(256)} %constant.15.clone.1), kind=kCustom, calls=%fused_computation.23 | custom fusion | bytes 1966592 | tf_op jit(solution)/shard_map/scatter | solution.py:81
  47.5 2.5 reshape.188
  50.0 124.9 %all_to_all.64 = bf16[32,60,512]{2,1,0:T(8,128)(2,1)} all-to-all(bf16[32,60,512]{2,1,0:T(8,128)(2,1)S(1)} %reshape.188), channel_id=1, replica_groups=mesh['grp'=2,'fs_0'=16,'fs_1'=2,'tp'=4] {'fs_0','fs_1'}, dimensions={0} | all-to-all | bytes 3932160 | tf_op jit(solution)/shard_map/all_to_all | solution.py:83
  174.9 3.9 all_to_all.55
  181.4 116.5 %all_to_all.65 = bf16[32,64,512]{2,1,0:T(8,128)(2,1)S(1)} all-to-all(bf16[32,64,512]{2,1,0:T(8,128)(2,1)S(1)} %pad_maximum_fusion), channel_id=1, replica_groups=mesh['grp'=2,'fs_0'=16,'fs_1'=2,'tp'=4] {'fs_0','fs_1'}, dimensions={0} | all-to-all | bytes 4194304 | tf_op jit(solution)/shard_map/all_to_all | solution.py:18
  298.0 6.2 %fusion.7 = f32[1920,256]{1,0:T(8,128)S(1)} fusion(bf16[1,1920,2048]{2,1,0:T(8,128)(2,1)} %all-gather.4.cloned.1.call-done, bf16[1,2048,256]{2,1,0:T(8,128)(2,1)S(1)} %get-tuple-element.17), kind=kOutput, calls=%fused_computation.15 | convolution fusion | flops 2013757440 | bytes 10878976 | tf_op jit(solution)/shard_map/erd,edf->erf/dot_general | solution.py:87
  304.3 3.6 fusion.19
  308.1 59.6 %all_to_all.66 = bf16[32,32,512]{2,1,0:T(8,128)(2,1)S(1)} all-to-all(bf16[32,32,512]{2,1,0:T(8,128)(2,1)S(1)} %convert_element_type.76), channel_id=1, replica_groups=mesh['grp'=2,'fs_0'=16,'fs_1'=2,'tp'=4] {'fs_0','fs_1'}, dimensions={0} | all-to-all | bytes 2097152 | tf_op jit(solution)/shard_map/all_to_all | solution.py:59
  369.9 8.0 %reduce.4 = bf16[1024,512]{1,0:T(8,128)(2,1)} reduce(bf16[1024,1,512]{2,1,0:T(2,128)(2,1)S(1)} %bitcast.86, bf16[]{:T(256)} %broadcast.145), dimensions={1}, to_apply=%bitcast.77.reduce_sub_computation | reduce | bytes 2097154
  377.9 3.7 reshape.234
  386.3 2.4 add_convert_fusion
  388.6 2.6 reshape_transpose_reshape.3
  392.4 5.3 all_to_all.67
  397.7 4.6 all-to-all-start.2
  402.3 3.3 copy.45
  405.6 12.1 %all-to-all-done.2 = bf16[4,2,65536]{2,1,0:T(2,128)(2,1)S(1)} async-done(((bf16[4,2,65536]{2,1,0:T(2,128)(2,1)}), bf16[4,2,65536]{2,1,0:T(2,128)(2,1)S(1)}, u32[]{:S(2)}, u32[]{:S(2)}) %all-to-all-start.2) | async-done | bytes 1048608 | tf_op jit(solution)/shard_map/all_to_all | solution.py:61
  417.7 4.8 all-to-all-start.5
  425.9 86.9 %all-to-all-done.5 = bf16[16,2,1,60,512]{4,1,3,2,0:T(2,128)(2,1)} async-done(((bf16[16,2,1,60,512]{4,1,3,2,0:T(2,128)(2,1)}), bf16[16,2,1,60,512]{4,1,3,2,0:T(2,128)(2,1)}, u32[]{:S(2)}, u32[]{:S(2)}) %all-to-all-start.5) | async-done | bytes 1966112 | tf_op jit(solution)/shard_map/all_to_all | solution.py:43
  512.8 3.3 copy.46
  516.1 2.5 reshape_reshape_reshape.3
  518.6 5.4 %gather_fusion = bf16[1536,512]{1,0:T(8,128)(2,1)} fusion(bf16[1920,512]{1,0:T(8,128)(2,1)S(1)} %reshape_reshape_reshape.3, s32[2048]{0:T(1024)S(1)} %pad_clamp_fusion), kind=kCustom, calls=%fused_computation.1 | custom fusion | bytes 3151872 | tf_op jit(solution)/shard_map/gather | solution.py:105
  524.1 2.8 reshape.200
  526.8 3.2 multiply_reduce_fusion
  (62 shorter events, 22.6 us)
Async XLA Ops:
  7.2 290.9 %all-gather.4.cloned.1.call-start = ((), (), s32[]{:S(2)}) async-start(), calls=%async_computation.6 | async-start | bytes 9830400 | tf_op jit(solution)/shard_map/all_gather | solution.py:86
  7.2 1.9 copy-start
  7.3 2.3 copy-start.6
  174.9 4.1 copy-start.2
  174.9 4.1 copy-start.8
  178.9 202.7 %all-gather.6.cloned.1.call-start = ((), (), s32[]{:S(2)}) async-start(), calls=%async_computation.7 | async-start | bytes 4915200 | tf_op jit(solution)/shard_map/all_gather | solution.py:95
  298.0 6.3 %copy-start.5 = (bf16[1,2048,256]{2,1,0:T(8,128)(2,1)}, bf16[1,2048,256]{2,1,0:T(8,128)(2,1)S(1)}, u32[]{:S(2)}) copy-start(bf16[1,2048,256]{2,1,0:T(8,128)(2,1)S(1)} %get-tuple-element.17) | copy-start | bytes 3145732
  298.0 6.3 %copy-start.4 = (bf16[1,2048,256]{2,1,0:T(8,128)(2,1)}, bf16[1,2048,256]{2,1,0:T(8,128)(2,1)S(1)}, u32[]{:S(2)}) copy-start(bf16[1,2048,256]{2,1,0:T(8,128)(2,1)S(1)} %get-tuple-element.16) | copy-start | bytes 3145732
  298.0 6.2 %copy-start.9 = (bf16[1,1920,2048]{2,1,0:T(8,128)(2,1)S(1)}, bf16[1,1920,2048]{2,1,0:T(8,128)(2,1)}, u32[]{:S(2)}) copy-start(bf16[1,1920,2048]{2,1,0:T(8,128)(2,1)} %all-gather.4.cloned.1.call-done) | copy-start | bytes 23592964
  304.3 3.7 copy-start.3
  381.7 3.9 copy-start.1
  397.7 20.0 %all-to-all-start.2 = ((bf16[4,2,65536]{2,1,0:T(2,128)(2,1)}), bf16[4,2,65536]{2,1,0:T(2,128)(2,1)S(1)}, u32[]{:S(2)}, u32[]{:S(2)}) async-start(bf16[4,2,65536]{2,1,0:T(2,128)(2,1)} %reshape.234), calls=%async_computation.2 | async-start | bytes 2097152 | tf_op jit(solution)/shard_map/all_to_all | solution.py:61
  405.6 16.9 %copy-start.7 = (f32[384,4]{0,1:T(4,128)S(1)}, f32[384,4]{0,1:T(4,128)}, u32[]{:S(2)}) copy-start(f32[384,4]{0,1:T(4,128)} %param.9) | copy-start | bytes 18436
  417.7 95.2 %all-to-all-start.5 = ((bf16[16,2,1,60,512]{4,1,3,2,0:T(2,128)(2,1)}), bf16[16,2,1,60,512]{4,1,3,2,0:T(2,128)(2,1)}, u32[]{:S(2)}, u32[]{:S(2)}) async-start(bf16[16,2,1,60,512]{4,1,3,2,0:T(2,128)(2,1)} %copy.45), calls=%async_computation.5 | async-start | bytes 3932160 | tf_op jit(solution)/shard_map/all_to_all | solution.py:43
Sparse Core Ops, SparseCore 0:
  179.0 76.8 all-gather.3
  308.1 46.6 all-gather.5
where the time goes:
time: 547 us; the launch traced here: 537 us
  blocking collectives  306 us (56%)
  waiting for transfers between devices  99.1 us (18%)
  local copies, waits for them, and re-layouts  55.4 us (10%)
  other arithmetic  35.3 us (6%)
  matrix products  16.7 us (3%)
  between operations  14.8 us (3%)
  starting transfers between devices  9.51 us (2%)
    all_to_all x1, blocking collectives, shards(): lax.all_to_all(outbox.reshape(experts, capacity, quarter), FS, split_axis...  125 us
    all_to_all x1, blocking collectives, in_one_piece(): lax.all_to_all(both, axis, split_axis=split_dim, concat_axis=concat_dim,...  116 us
    all_to_all x1, waiting for transfers between devices, moved_by_axis(): out = lax.all_to_all(out, axes[k], k, k, tiled=True)  86.9 us
    all_to_all x1, blocking collectives, shards(): lax.all_to_all(down_cast, FS, split_axis=0, concat_axis=1, tiled=True)  59.6 us
    another operation x3, other arithmetic  16.8 us
    scatter x1, local copies, waits for them, and re-layouts, shards(): jnp.zeros((experts * capacity, quarter), jnp.bfloat16).at[target]  15.8 us
    all_to_all x1, waiting for transfers between devices, shards(): lax.all_to_all(down_rows, 'tp', split_axis=1, concat_axis=2, tiled=True)  12.1 us
  transfers between devices with their start and end apart: 4, of which 2 were waited for; matrix products, arithmetic and copies ran while one was open for 4% of the time, Pallas kernels for 0%

commit v1 on v0

--- a/solution.py
+++ b/solution.py
@@ -10,6 +10,12 @@
 LIMIT = 7.0
 ALPHA = 1.702
 EPS = 1e-06
+
+
+def exchange_blocks(x, axis, split, join):
+    pieces = jnp.split(x, lax.axis_size(axis), axis=split)
+    got = lax.all_to_all(jnp.stack(pieces), axis, 0, 0)
+    return jnp.concatenate(got, axis=join)
 
 
 def in_one_piece(arrays, axis, split_dim, concat_dim, along):
@@ -56,7 +62,7 @@
     down_cast = down_train.astype(jnp.bfloat16)
     gate_mine, up_mine, down_rows = (
         *in_one_piece((gate_cast, up_cast), FS, 0, 1, 2),
-        lax.all_to_all(down_cast, FS, split_axis=0, concat_axis=1, tiled=True),
+        exchange_blocks(down_cast, FS, 0, 1),
     )
     down_mine = lax.all_to_all(down_rows, "tp", split_axis=1, concat_axis=2, tiled=True)
     tok_rows, width = prompt.shape

time: 547 us -> 545 us (level)
  blocking collectives: 306 us -> 191 us
  waiting for transfers between devices: 99.1 us -> 171 us
  local copies, waits for them, and re-layouts: 55.4 us -> 76.7 us
  starting transfers between devices: 9.51 us -> 26.7 us
    all_to_all x2 -> x1, blocking collectives: 176 us -> 60.5 us  [exchange_blocks(): got = lax.all_to_all(jnp.stack(pieces), axis, 0, 0)]
    all_to_all x0 -> x1, waiting for transfers between devices: none -> 72.3 us  [in_one_piece(): lax.all_to_all(both, axis, split_axis=split_dim, concat_axis=concat_dim,...]
    unnamed x27 -> x54, local copies, waits for them, and re-layouts: 7.25 us -> 26.6 us
    all_gather x1, starting transfers between devices: 0.07 us -> 12.3 us  [shards(): piece = lax.all_gather(hidden, 'tp', axis=2, tiled=True)]
  transfers between devices with their start and end apart: 4 -> 5, of which waited for: 2 -> 3; matrix products, arithmetic and copies ran while one was open for 4% -> 9% of each run, Pallas kernels for 0% -> 0%
where the time goes in v1:
time: 545 us; the launch traced here: 535 us
  blocking collectives  191 us (35%)
  waiting for transfers between devices  171 us (31%)
  local copies, waits for them, and re-layouts  76.7 us (14%)
  other arithmetic  38.4 us (7%)
  starting transfers between devices  26.7 us (5%)
  matrix products  16.3 us (3%)
  between operations  14.8 us (3%)
    all_to_all x1, blocking collectives, shards(): lax.all_to_all(outbox.reshape(experts, capacity, quarter), FS, split_axis...  125 us
    all_to_all x1, waiting for transfers between devices, moved_by_axis(): out = lax.all_to_all(out, axes[k], k, k, tiled=True)  86.9 us
    all_to_all x1, waiting for transfers between devices, in_one_piece(): lax.all_to_all(both, axis, split_axis=split_dim, concat_axis=concat_dim,...  72.3 us
    all_to_all x1, blocking collectives, exchange_blocks(): got = lax.all_to_all(jnp.stack(pieces), axis, 0, 0)  60.5 us
    unnamed x54, local copies, waits for them, and re-layouts  26.6 us
    another operation x3, other arithmetic  16.8 us
    scatter x1, local copies, waits for them, and re-layouts, shards(): jnp.zeros((experts * capacity, quarter), jnp.bfloat16).at[target]  15.8 us
    all_gather x1, starting transfers between devices, shards(): piece = lax.all_gather(hidden, 'tp', axis=2, tiled=True)  12.3 us
  transfers between devices with their start and end apart: 5, of which 3 were waited for; matrix products, arithmetic and copies ran while one was open for 9% of the time, Pallas kernels for 0%

profile of v1, /device:TPU:40, one launch (start us, length us, event | category | flops | bytes accessed | tf_op | source)
XLA Modules:
  0.0 535.1 jit_solution(4909778127345454928)
XLA Ops:
  10.8 15.9 %reduce-window.6 = s32[32,12,128]{2,1,0:T(8,128)S(1)} reduce-window(s32[32,12,128]{2,1,0:T(8,128)} %fusion.28, s32[]{:T(128)} %constant.22.clone.1), window={size=1x1x128 pad=0_0x0_0x127_0}, to_apply=%region_0.0 | reduce-window | flops 6242304 | bytes 393220 | tf_op jit(solution)/shard_map/reduce-window
  31.7 15.8 %scatter_custom_fusion = bf16[1920,512]{1,0:T(8,128)(2,1)} fusion(s32[1536]{0:T(1024)S(1)} %fusion.32, bf16[384,512]{1,0:T(8,128)(2,1)S(1)} %fusion.27, s32[2048]{0:T(1024)} %pad_clamp_fusion.1, bf16[]{:T(256)} %constant.15.clone.1), kind=kCustom, calls=%fused_computation.23 | custom fusion | bytes 1966592 | tf_op jit(solution)/shard_map/scatter | solution.py:87
  50.0 124.9 %all_to_all.57 = bf16[32,60,512]{2,1,0:T(8,128)(2,1)} all-to-all(bf16[32,60,512]{2,1,0:T(8,128)(2,1)S(1)} %reshape.189), channel_id=1, replica_groups=mesh['grp'=2,'fs_0'=16,'fs_1'=2,'tp'=4] {'fs_0','fs_1'}, dimensions={0} | all-to-all | bytes 3932160 | tf_op jit(solution)/shard_map/all_to_all | solution.py:89
  174.9 3.9 all_to_all.48
  182.7 4.9 all-to-all-start
  187.6 12.3 %all-gather.6.cloned.1.call-start = ((), (), s32[]{:S(2)}) async-start(), calls=%async_computation.7 | async-start | bytes 4915200 | tf_op jit(solution)/shard_map/all_gather | solution.py:101
  215.9 72.3 %all-to-all-done = bf16[32,64,512]{2,1,0:T(8,128)(2,1)S(1)} async-done(((bf16[32,64,512]{2,1,0:T(8,128)(2,1)}), bf16[32,64,512]{2,1,0:T(8,128)(2,1)S(1)}, u32[]{:S(2)}, u32[]{:S(2)}) %all-to-all-start) | async-done | bytes 2097184 | tf_op jit(solution)/shard_map/all_to_all | solution.py:24
  289.7 5.8 %fusion.7 = f32[1920,256]{1,0:T(8,128)S(1)} fusion(bf16[1,1920,2048]{2,1,0:T(8,128)(2,1)} %all-gather.4.cloned.1.call-done, bf16[1,2048,256]{2,1,0:T(8,128)(2,1)} %get-tuple-element.21), kind=kOutput, calls=%fused_computation.15 | convolution fusion | flops 2013757440 | bytes 10878976 | tf_op jit(solution)/shard_map/erd,edf->erf/dot_general | solution.py:93
  295.8 3.6 fusion.19
  305.0 60.5 %all_to_all.58 = bf16[32,1,32,512]{3,2,1,0:T(8,128)(2,1)S(1)} all-to-all(bf16[32,1,32,512]{3,2,1,0:T(8,128)(2,1)} %constant_dynamic-update-slice_fusion), channel_id=1, replica_groups=mesh['grp'=2,'fs_0'=16,'fs_1'=2,'tp'=4] {'fs_0','fs_1'}, dimensions={0} | all-to-all | bytes 2097152 | tf_op jit(solution)/shard_map/all_to_all | solution.py:17
  367.7 8.0 %reduce.4 = bf16[1024,512]{1,0:T(8,128)(2,1)} reduce(bf16[1024,1,512]{2,1,0:T(2,128)(2,1)S(1)} %bitcast.214, bf16[]{:T(256)} %broadcast.145), dimensions={1}, to_apply=%bitcast.205.reduce_sub_computation | reduce | bytes 2097154
  375.7 3.7 reshape.235
  386.4 2.6 reshape_transpose_reshape.3
  390.2 5.3 all_to_all.59
  395.5 4.6 all-to-all-start.2
  400.1 3.3 copy.88
  403.4 12.1 %all-to-all-done.2 = bf16[4,2,65536]{2,1,0:T(2,128)(2,1)S(1)} async-done(((bf16[4,2,65536]{2,1,0:T(2,128)(2,1)}), bf16[4,2,65536]{2,1,0:T(2,128)(2,1)S(1)}, u32[]{:S(2)}, u32[]{:S(2)}) %all-to-all-start.2) | async-done | bytes 1048608 | tf_op jit(solution)/shard_map/all_to_all | solution.py:67
  415.5 4.8 all-to-all-start.5
  423.7 86.9 %all-to-all-done.5 = bf16[16,2,1,60,512]{4,1,3,2,0:T(2,128)(2,1)} async-done(((bf16[16,2,1,60,512]{4,1,3,2,0:T(2,128)(2,1)}), bf16[16,2,1,60,512]{4,1,3,2,0:T(2,128)(2,1)}, u32[]{:S(2)}, u32[]{:S(2)}) %all-to-all-start.5) | async-done | bytes 1966112 | tf_op jit(solution)/shard_map/all_to_all | solution.py:49
  510.6 3.3 copy.89
  514.0 2.5 reshape_reshape_reshape.3
  516.5 5.4 %gather_fusion = bf16[1536,512]{1,0:T(8,128)(2,1)} fusion(bf16[1920,512]{1,0:T(8,128)(2,1)S(1)} %reshape_reshape_reshape.3, s32[2048]{0:T(1024)S(1)} %pad_clamp_fusion), kind=kCustom, calls=%fused_computation.1 | custom fusion | bytes 3151872 | tf_op jit(solution)/shard_map/gather | solution.py:111
  521.9 2.8 reshape.201
  524.7 3.2 multiply_reduce_fusion
  (91 shorter events, 51.6 us)
Async XLA Ops:
  7.2 282.5 %all-gather.4.cloned.1.call-start = ((), (), s32[]{:S(2)}) async-start(), calls=%async_computation.6 | async-start | bytes 9830400 | tf_op jit(solution)/shard_map/all_gather | solution.py:92
  7.2 1.9 copy-start
  7.3 2.3 copy-start.4
  174.9 4.0 copy-start.2
  174.9 4.0 copy-start.6
  182.7 105.6 %all-to-all-start = ((bf16[32,64,512]{2,1,0:T(8,128)(2,1)}), bf16[32,64,512]{2,1,0:T(8,128)(2,1)S(1)}, u32[]{:S(2)}, u32[]{:S(2)}) async-start(bf16[32,64,512]{2,1,0:T(8,128)(2,1)} %pad_maximum_fusion), calls=%async_computation | async-start | bytes 4194304 | tf_op jit(solution)/shard_map/all_to_all | solution.py:24
  187.6 191.9 %all-gather.6.cloned.1.call-start = ((), (), s32[]{:S(2)}) async-start(), calls=%async_computation.7 | async-start | bytes 4915200 | tf_op jit(solution)/shard_map/all_gather | solution.py:101
  289.7 5.8 %copy-start.3 = (bf16[1,2048,256]{2,1,0:T(8,128)(2,1)S(1)}, bf16[1,2048,256]{2,1,0:T(8,128)(2,1)}, u32[]{:S(2)}) copy-start(bf16[1,2048,256]{2,1,0:T(8,128)(2,1)} %get-tuple-element.20) | copy-start | bytes 3145732
  289.7 6.1 %copy-start.7 = (bf16[1,1920,2048]{2,1,0:T(8,128)(2,1)S(1)}, bf16[1,1920,2048]{2,1,0:T(8,128)(2,1)}, u32[]{:S(2)}) copy-start(bf16[1,1920,2048]{2,1,0:T(8,128)(2,1)} %all-gather.4.cloned.1.call-done) | copy-start | bytes 23592964
  379.5 3.9 copy-start.1
  395.5 20.0 %all-to-all-start.2 = ((bf16[4,2,65536]{2,1,0:T(2,128)(2,1)}), bf16[4,2,65536]{2,1,0:T(2,128)(2,1)S(1)}, u32[]{:S(2)}, u32[]{:S(2)}) async-start(bf16[4,2,65536]{2,1,0:T(2,128)(2,1)} %reshape.235), calls=%async_computation.2 | async-start | bytes 2097152 | tf_op jit(solution)/shard_map/all_to_all | solution.py:67
  403.4 16.9 %copy-start.5 = (f32[384,4]{0,1:T(4,128)S(1)}, f32[384,4]{0,1:T(4,128)}, u32[]{:S(2)}) copy-start(f32[384,4]{0,1:T(4,128)} %param.9) | copy-start | bytes 18436
  415.5 95.2 %all-to-all-start.5 = ((bf16[16,2,1,60,512]{4,1,3,2,0:T(2,128)(2,1)}), bf16[16,2,1,60,512]{4,1,3,2,0:T(2,128)(2,1)}, u32[]{:S(2)}, u32[]{:S(2)}) async-start(bf16[16,2,1,60,512]{4,1,3,2,0:T(2,128)(2,1)} %copy.88), calls=%async_computation.5 | async-start | bytes 3932160 | tf_op jit(solution)/shard_map/all_to_all | solution.py:49
Sparse Core Ops, SparseCore 0:
  179.0 76.8 all-gather.3
  299.6 46.9 all-gather.5
